TPU v7x, 256 devices: a 2x2x32 block of a 4x8x32 slice. The times are simulated.
256 devices in a mesh: grp: 4 (over y, x), ep: 64 (over z, core).
Axes of the slice: x: 2, y: 2, z: 32, core: 2. Of those that a mesh axis runs over, the one named last changes fastest.
The devices are a block of a 4x8x32 slice.
Arguments:
- tokens: bfloat16 [1024, 2048], P(('grp', 'ep')), parts along dimension 0, may hold values from -6 to 6
- lengths: int32 [1024], P(('grp', 'ep')), parts along dimension 0, may hold values from 128 to 1024, as said below
- cache_key: bfloat16 [1024, 1024, 256], P(('grp', 'ep')), parts along dimension 0, may hold values from -6 to 6
- cache_value: bfloat16 [1024, 1024, 256], P(('grp', 'ep')), parts along dimension 0, may hold values from -6 to 6
- routes: int32 [1024, 2], P(('grp', 'ep')), parts along dimension 0, may hold values from 0 to 3, all different within a row
- route_logits: float32 [1024, 2], P(('grp', 'ep')), parts along dimension 0, may hold values from -6 to 6
- mix_gain: float32 [2048], replicated, may hold values from 0.1 to 1.9
- query_gain: float32 [64], replicated, may hold values from 0.1 to 1.9
- key_gain: float32 [64], replicated, may hold values from 0.1 to 1.9
- head_bias: float32 [16], replicated, may hold values from -9 to -3.5
- w_query: bfloat16 [2048, 1024], P('ep'), may hold values from -0.125 to 0.125
- w_key: bfloat16 [2048, 256], P('ep'), may hold values from -0.125 to 0.125
- w_value: bfloat16 [2048, 256], P('ep'), may hold values from -0.125 to 0.125
- w_out: bfloat16 [1024, 2048], P(None, 'ep'), may hold values from -0.1875 to 0.1875
- ffn_gain: float32 [2048], replicated, may hold values from 0.1 to 1.9
- w_gate: bfloat16 [2048, 28672], P(None, 'ep'), may hold values from -0.125 to 0.125
- w_up: bfloat16 [2048, 28672], P(None, 'ep'), may hold values from -0.125 to 0.125
- w_down: bfloat16 [28672, 2048], P('ep'), may hold values from -0.0625 to 0.0625
Outputs:
- output: bfloat16 [1024, 2048], P(('grp', 'ep')), parts along dimension 0
- new_key: bfloat16 [1024, 256], P(('grp', 'ep')), parts along dimension 0
- new_value: bfloat16 [1024, 256], P(('grp', 'ep')), parts along dimension 0
There are 4 independent parts, one for each index of `grp`. A program takes and returns all parts, laid end to end along the dimension named above; an argument that names none is the same for every part. Nothing has to cross between parts.
Inputs may be any that keep to these rules, and one draw needn't show every extreme that they name: `lengths`: some sequence has all 1024 positions live.
All inputs are finite; a program needn't handle non-finite values.
Results may differ from a plain program's by a relative error of at most 0.0085.
Values may be sent and summed in bfloat16 or wider, within the bound.
A program may use at most 128 MiB of HBM per device.

v0:
```python
import jax
import jax.numpy as jnp
from jax import lax
from jax.sharding import Mesh
from jax.sharding import PartitionSpec as P

HEADS = 16
KV_HEADS = 4
HEAD_DIM = 64
FF = 7168
EXPERTS = 4
EP = ("ep_0", "ep_1")
GRP_EP = ("grp", "ep_0", "ep_1")


EPSILON = 1e-06


def in_one_piece(arrays, axis, dim, along):
    both = jnp.concatenate(arrays, axis=along)
    whole, at, gathered = (lax.all_gather(both, axis, axis=dim, tiled=True), 0, [])
    for a in arrays:
        gathered.append(lax.slice_in_dim(whole, at, at + a.shape[along], axis=along))
        at += a.shape[along]
    return tuple(gathered)


def sent_to_all(array, axis):
    copies = jnp.broadcast_to(array, (lax.axis_size(axis), *array.shape))
    return lax.all_to_all(copies, axis, split_axis=0, concat_axis=0, tiled=True)


def laid_out(blocks, dim):
    blocks = jnp.moveaxis(blocks, 0, dim)
    dims = blocks.shape
    return blocks.reshape(*dims[:dim], dims[dim] * dims[dim + 1], *dims[dim + 2 :])


def collect(array, axis, dim):
    blocks = sent_to_all(array, axis)
    return laid_out(blocks, dim)


def all_blocks(array, axes, turns):
    blocks = array
    for k in turns:
        blocks = lax.all_gather(blocks, axes[k])
    done = turns[::-1]
    back = [done.index(k) for k in range(len(axes))]
    blocks = blocks.transpose(*back, *range(len(axes), blocks.ndim))
    return blocks.reshape(-1, *array.shape)


def gathered_by_axis(array, axes, turns, dim):
    return laid_out(all_blocks(array, axes, turns), dim)


def sum_in_order(blocks, axes, turns):
    dims = [lax.axis_size(a) for a in axes]
    blocks = blocks.reshape(*dims, *blocks.shape[1:])
    blocks = blocks.transpose(*turns, *range(len(axes), blocks.ndim))
    blocks = blocks.reshape(-1, *blocks.shape[len(axes) :])
    for k in turns:
        blocks = lax.psum_scatter(blocks, axes[k], scatter_dimension=0, tiled=True)
    return blocks[0]


def in_blocks(array, dim, count):
    before, after = (array.shape[:dim], array.shape[dim + 1 :])
    return jnp.moveaxis(array.reshape(*before, count, -1, *after), dim, 0)


def sum_by_axis(array, axes, turns, dim):
    count = lax.axis_size(axes)
    return sum_in_order(in_blocks(array, dim, count), axes, turns)


def rms_scaled(values, gain):
    return values * lax.rsqrt(jnp.mean(values * values, axis=-1, keepdims=True) + EPSILON) * gain


def route_weights(routes, route_logits):
    experts_iota = jnp.arange(EXPERTS, dtype=jnp.int32)[None, :]
    first_share = jax.nn.sigmoid(route_logits[:, 0:1] - route_logits[:, 1:2])
    second_share = jax.nn.sigmoid(route_logits[:, 1:2] - route_logits[:, 0:1])
    return jnp.where(routes[:, 0:1] == experts_iota, first_share, 0.0) + jnp.where(
        routes[:, 1:2] == experts_iota, second_share, 0.0
    )


def stick_attend(queries, lengths, cache_key, cache_value, query_gain, head_bias):
    batch_rows = queries.shape[0]
    cache_len = cache_key.shape[1]
    group_size = HEADS // KV_HEADS
    normed_query = rms_scaled(queries.reshape(batch_rows, HEADS, HEAD_DIM), query_gain).astype(
        jnp.bfloat16
    )
    normed_query = normed_query.reshape(batch_rows, KV_HEADS, group_size, HEAD_DIM)
    key_heads = cache_key.reshape(batch_rows, cache_len, KV_HEADS, HEAD_DIM)
    value_heads = cache_value.reshape(batch_rows, cache_len, KV_HEADS, HEAD_DIM)
    scores = jnp.einsum(
        "bkgd,blkd->bkgl", normed_query, key_heads, preferred_element_type=jnp.float32
    ) * HEAD_DIM ** (-0.5)
    scores = scores + head_bias.reshape(KV_HEADS, group_size)[None, :, :, None]
    live_mask = (
        jnp.arange(cache_len, dtype=jnp.int32)[None, None, None, :] < lengths[:, None, None, None]
    )
    remain = jnp.where(live_mask, jax.nn.log_sigmoid(-scores), 0.0)
    after_sum = lax.cumsum(remain, axis=3, reverse=True) - remain
    weights = jnp.where(live_mask, jnp.exp(jax.nn.log_sigmoid(scores) + after_sum), 0.0).astype(
        jnp.bfloat16
    )
    attended = jnp.einsum(
        "bkgl,blkd->bkgd", weights, value_heads, preferred_element_type=jnp.float32
    )
    return attended.reshape(batch_rows, HEADS * HEAD_DIM).astype(jnp.bfloat16)


def local(
    tokens,
    lengths,
    cache_key,
    cache_value,
    routes,
    route_logits,
    mix_gain,
    query_gain,
    key_gain,
    head_bias,
    w_query,
    w_key,
    w_value,
    w_out,
    ffn_gain,
    w_gate,
    w_up,
    w_down,
):
    token_rows = tokens.shape[0]
    key_width = w_key.shape[1]
    as_float = tokens.astype(jnp.float32)
    normed = rms_scaled(as_float, mix_gain).astype(jnp.bfloat16)
    pieces = in_one_piece((w_query, w_key, w_value), EP, 0, 1)
    queries, fresh_key, fresh_value = tuple(
        (jnp.dot(normed, weight, preferred_element_type=jnp.float32) for weight in pieces)
    )
    new_key = rms_scaled(fresh_key.reshape(token_rows, KV_HEADS, HEAD_DIM), key_gain)
    new_key = new_key.reshape(token_rows, key_width).astype(jnp.bfloat16)
    new_value = fresh_value.astype(jnp.bfloat16)
    attended = stick_attend(queries, lengths, cache_key, cache_value, query_gain, head_bias)
    mixed = as_float + jnp.dot(
        attended, lax.all_gather(w_out, EP, axis=1, tiled=True), preferred_element_type=jnp.float32
    )
    expert_in = rms_scaled(mixed, ffn_gain).astype(jnp.bfloat16)
    every_gate = collect(route_weights(routes, route_logits), EP, 0)
    ff_share = w_gate.shape[1]
    my_expert = lax.axis_index(EP) // (FF // ff_share)
    my_gate = lax.dynamic_slice_in_dim(every_gate, my_expert, 1, 1)
    input_rows = gathered_by_axis(expert_in, EP, (0, 1), 0)
    gate_value = jnp.dot(input_rows, w_gate, preferred_element_type=jnp.float32)
    up_value = jnp.dot(input_rows, w_up, preferred_element_type=jnp.float32)
    hidden = (jax.nn.silu(gate_value) * up_value * my_gate).astype(jnp.bfloat16)
    expert_sum = sum_by_axis(
        jnp.dot(hidden, w_down, preferred_element_type=jnp.float32), EP, (1, 0), 0
    )
    return ((mixed + expert_sum).astype(jnp.bfloat16), new_key, new_value)


def solution(mesh):
    finer = Mesh(mesh.devices.reshape(mesh.shape["grp"], 32, 2), ("grp", "ep_0", "ep_1"))
    in_specs = (
        P(GRP_EP, None),
        P(GRP_EP),
        P(GRP_EP, None, None),
        P(GRP_EP, None, None),
        P(GRP_EP, None),
        P(GRP_EP, None),
        P(),
        P(),
        P(),
        P(),
        P(EP, None),
        P(EP, None),
        P(EP, None),
        P(None, EP),
        P(),
        P(None, EP),
        P(None, EP),
        P(EP, None),
    )
    out_specs = (P(GRP_EP, None), P(GRP_EP, None), P(GRP_EP, None))
    return jax.shard_map(local, mesh=finer, in_specs=in_specs, out_specs=out_specs, check_vma=False)
```

profile of v0, /device:TPU:38, one launch (start us, length us, event | category | flops | bytes accessed | tf_op | source)
XLA Modules:
  0.0 721.5 jit_solution(17968655705185238945)
XLA Ops:
  7.3 1.6 pad_maximum_fusion
  9.9 4.0 copy.32
  13.9 4.0 copy.33
  18.1 139.9 %all-gather.7.cloned.1.call-done = bf16[2048,1536]{1,0:T(8,128)(2,1)} async-done(((bf16[32,1536]{1,0:T(8,128)(2,1)}), bf16[2048,1536]{1,0:T(8,128)(2,1)}) %all-gather.7.cloned.1.call-update) | async-done | bytes 6291472 | tf_op jit(solution)/shard_map/all_gather | solution.py:21
  158.0 2.9 fusion.40
  161.3 2.2 fusion.20
  163.6 79.2 %reduce-window.6 = f32[4,4,4,8,128]{4,3,2,1,0:T(8,128)S(1)} reduce-window(f32[4,4,4,8,128]{4,3,2,1,0:T(8,128)S(1)} %reshape.109, f32[]{:T(128)} %constant.24.clone.1), window={size=1x1x1x1x128 pad=0_0x0_0x0_0x0_0x0_127}, to_apply=%region_2.0 | reduce-window | flops 8323072 | bytes 524292 | tf_op jit(solution)/shard_map/reduce-window
  243.0 2.8 reduce-window.9
  246.2 2.5 convolution_convert_fusion
  248.9 36.8 %all-gather.9.cloned.1.call-done = bf16[1024,2048]{0,1:T(8,128)(2,1)} async-done(((bf16[1024,32]{0,1:T(8,128)(2,1)}), bf16[1024,2048]{0,1:T(8,128)(2,1)}) %all-gather.9.cloned.1.call-update) | async-done | bytes 4194320 | tf_op jit(solution)/shard_map/all_gather | solution.py:152
  285.7 3.5 multiply_reduce_fusion
  289.3 60.4 %all-gather.2 = bf16[32,4,2048]{2,1,0:T(4,128)(2,1)} all-gather(bf16[1,4,2048]{2,1,0:T(4,128)(2,1)S(1)} %fusion.31), channel_id=2, replica_groups=mesh['grp'=4,'ep_0'=32,'ep_1'=2] {'ep_0'}, dimensions={0}, use_global_device_ids=true | all-gather | bytes 540672 | tf_op jit(solution)/shard_map/all_gather | solution.py:47
  350.5 14.5 %all-to-all-start = ((f32[64,4,4]{1,2,0:T(4,128)}), f32[64,4,4]{1,2,0:T(4,128)S(1)}, u32[]{:S(2)}, u32[]{:S(2)}) async-start(f32[64,4,4]{1,2,0:T(4,128)} %broadcast_in_dim.56), calls=%async_computation | async-start | bytes 262144 | tf_op jit(solution)/shard_map/all_to_all | solution.py:30
  365.3 30.2 %all-to-all-done = f32[64,4,4]{1,2,0:T(4,128)S(1)} async-done(((f32[64,4,4]{1,2,0:T(4,128)}), f32[64,4,4]{1,2,0:T(4,128)S(1)}, u32[]{:S(2)}, u32[]{:S(2)}) %all-to-all-start) | async-done | bytes 4128 | tf_op jit(solution)/shard_map/all_to_all | solution.py:30
  395.6 2.8 copy.38
  399.8 2.2 fusion.42
  402.0 5.1 fusion.5
  407.2 2.9 reshape_reshape.7
  410.0 3.2 copy.36
  415.2 35.4 %all-reduce.5.cloned.1.call-done = f32[64,4,2048]{2,1,0:T(4,128)} async-done(((f32[64,4,2048]{2,1,0:T(4,128)}), f32[64,4,2048]{2,1,0:T(4,128)}) %all-reduce.5.cloned.1.call-update) | async-done | bytes 2097168
  450.6 2.4 constant_dynamic-slice_fusion
  456.1 2.1 convolution_convert_fusion.1
  458.2 254.8 %all-reduce.7.cloned.1.call-done = f32[32,4,2048]{2,1,0:T(4,128)} async-done(((f32[32,4,2048]{2,1,0:T(4,128)}), f32[32,4,2048]{2,1,0:T(4,128)}) %all-reduce.7.cloned.1.call-update) | async-done | bytes 1048592
  713.0 1.9 fusion.30
  (71 shorter events, 9.4 us)
Async XLA Ops:
  7.2 394.8 %copy-start = (bf16[448,2048]{1,0:T(8,128)(2,1)S(1)}, bf16[448,2048]{1,0:T(8,128)(2,1)}, u32[]{:S(2)}) copy-start(bf16[448,2048]{1,0:T(8,128)(2,1)} %param.35) | copy-start | bytes 5505028
  7.2 150.8 %all-gather.7.cloned.1.call-start = ((), (), s32[]{:S(2)}) async-start(), calls=%async_computation.1 | async-start | bytes 6389760 | tf_op jit(solution)/shard_map/all_gather | solution.py:21
  9.0 276.7 %all-gather.9.cloned.1.call-start = ((), (), s32[]{:S(2)}) async-start(), calls=%async_computation.2 | async-start | bytes 4259840 | tf_op jit(solution)/shard_map/all_gather | solution.py:152
  9.8 4.1 copy-start.6
  9.8 385.8 %all-gather.11.cloned.1.call-start = ((), (), s32[]{:S(2)}) async-start(), calls=%async_computation.3 | async-start | bytes 1572864 | tf_op jit(solution)/shard_map/all_gather | solution.py:47
  13.9 4.0 copy-start.1
  13.9 4.1 copy-start.7
  13.9 144.1 %copy-start.2 = (f32[2048]{0:T(1024)S(1)}, f32[2048]{0:T(1024)}, u32[]{:S(2)}) copy-start(f32[2048]{0:T(1024)} %param.24) | copy-start | bytes 24580
  18.1 143.1 %copy-start.9 = (f32[64]{0:T(128)S(1)}, f32[64]{0:T(128)}, u32[]{:S(2)}) copy-start(f32[64]{0:T(128)} %param.25) | copy-start | bytes 772
  248.8 40.4 %copy-start.3 = (f32[2048]{0:T(1024)S(1)}, f32[2048]{0:T(1024)}, u32[]{:S(2)}) copy-start(f32[2048]{0:T(1024)} %param.32) | copy-start | bytes 24580
  248.8 100.9 %copy-start.4 = (s32[4,2]{0,1:T(2,128)S(1)}, s32[4,2]{0,1:T(2,128)}, u32[]{:S(2)}) copy-start(s32[4,2]{0,1:T(2,128)} %param.22) | copy-start | bytes 100
  248.8 100.9 %copy-start.5 = (f32[4,2]{0,1:T(2,128)S(1)}, f32[4,2]{0,1:T(2,128)}, u32[]{:S(2)}) copy-start(f32[4,2]{0,1:T(2,128)} %param.23) | copy-start | bytes 100
  350.5 45.0 %all-to-all-start = ((f32[64,4,4]{1,2,0:T(4,128)}), f32[64,4,4]{1,2,0:T(4,128)S(1)}, u32[]{:S(2)}, u32[]{:S(2)}) async-start(f32[64,4,4]{1,2,0:T(4,128)} %broadcast_in_dim.56), calls=%async_computation | async-start | bytes 262144 | tf_op jit(solution)/shard_map/all_to_all | solution.py:30
  365.0 85.5 %all-reduce.5.cloned.1.call-start = ((), (), s32[]{:S(2)}) async-start(), calls=%async_computation.4 | async-start | bytes 4194304
  413.2 0.7 copy-start.11
  413.3 39.7 %copy-start.10 = (u32[256]{0:T(256)S(1)}, u32[256]{0:T(256)}, u32[]{:S(2)}) copy-start(u32[256]{0:T(256)} %constant.71) | copy-start | bytes 3076
  413.3 40.3 %copy-start.8 = (f32[64]{0:T(128)S(1)}, f32[64]{0:T(128)}, u32[]{:S(2)}) copy-start(f32[64]{0:T(128)} %param.26) | copy-start | bytes 772
  413.3 299.7 %all-reduce.7.cloned.1.call-start = ((), (), s32[]{:S(2)}) async-start(), calls=%async_computation.5 | async-start | bytes 2097152
Sparse Core Ops, SparseCore 0:
  9.9 148.1 all-gather.6
  159.9 125.7 all-gather.8
  349.9 17.5 all-gather.10
  413.4 37.0 all-reduce.4
  453.1 259.8 all-reduce.6
where the time goes:
time: 722 us; the launch traced here: 721 us
  waiting for transfers between devices  498 us (69%)
  other arithmetic  86.9 us (12%)
  blocking collectives  60.4 us (8%)
  local copies, waits for them, and re-layouts  24.4 us (3%)
  matrix products  22 us (3%)
  starting transfers between devices  15 us (2%)
  between operations  14.7 us (2%)
    unnamed x7, waiting for transfers between devices  291 us
    all_gather x1, waiting for transfers between devices, in_one_piece(): lax.all_gather(both, axis, axis=dim, tiled=True)  140 us
    another operation x2, other arithmetic  82.1 us
    all_gather x1, blocking collectives, all_blocks(): blocks = lax.all_gather(blocks, axes[k])  60.4 us
    all_gather x1, waiting for transfers between devices, local(): lax.all_gather(w_out, EP, axis=1, tiled=True)  36.8 us
    all_to_all x1, waiting for transfers between devices, sent_to_all(): return lax.all_to_all(copies, axis, split_axis=0, concat_axis=0, tiled=True)  30.2 us
    all_to_all x1, starting transfers between devices, sent_to_all(): return lax.all_to_all(copies, axis, split_axis=0, concat_axis=0, tiled=True)  14.5 us
  transfers between devices with their start and end apart: 6, of which 5 were waited for; matrix products, arithmetic and copies ran while one was open for 15% of the time, Pallas kernels for 0%

commit v1 on v0

v1 whole, which is shorter than its diff:
```python
import functools

import jax
import jax.numpy as jnp
from jax import lax
from jax.experimental import pallas as pl
from jax.experimental.pallas import tpu as pltpu
from jax.sharding import PartitionSpec as P

HEADS = 16
KV_HEADS = 4
GROUP = HEADS // KV_HEADS
HEAD_DIM = 64
FF = 7168
EXPERTS = 4
EP = "ep"
NEAR = 4
LANES = 128
EPSILON = 1e-06
F32 = jnp.float32
BF16 = jnp.bfloat16
MESH = pl.DeviceIdType.MESH


def rms_scaled(values, gain):
    return values * lax.rsqrt(jnp.mean(values * values, axis=-1, keepdims=True) + EPSILON) * gain


def route_weights(routes, route_logits):
    experts_iota = jnp.arange(EXPERTS, dtype=jnp.int32)[None, :]
    first_share = jax.nn.sigmoid(route_logits[:, 0:1] - route_logits[:, 1:2])
    second_share = jax.nn.sigmoid(route_logits[:, 1:2] - route_logits[:, 0:1])
    return jnp.where(routes[:, 0:1] == experts_iota, first_share, 0.0) + jnp.where(
        routes[:, 1:2] == experts_iota, second_share, 0.0
    )


def remote(src, dst, send_sem, recv_sem, device):
    return pltpu.make_async_remote_copy(
        src_ref=src,
        dst_ref=dst,
        send_sem=send_sem,
        recv_sem=recv_sem,
        device_id={EP: device},
        device_id_type=MESH,
    )


def greet(devices):
    barrier = pltpu.get_barrier_semaphore()
    for device in devices:
        pl.semaphore_signal(barrier, inc=1, device_id={EP: device}, device_id_type=MESH)
    pl.semaphore_wait(barrier, len(devices))


def place(chips):
    me = lax.axis_index(EP)
    z, core = lax.div(me, 2), lax.rem(me, 2)

    def at(chip, c):
        return lax.rem(chip + 2 * chips, chips) * 2 + c

    return z, core, at


def ring_kernel(chips, x_ref, wa_ref, wb_ref, qkv_ref, wb_out, a_buf, b_buf, s_send, s_recv, p_send, p_recv, o_sem):
    z, core, at = place(chips)
    right, left, partner = at(z + 1, core), at(z - 1, core), at(z, 1 - core)
    rows = wa_ref.shape[0]
    half = chips // 2
    limits = (half, half - 1)
    bufs = (a_buf, b_buf)
    greet((left, right, partner))
    loads = [pltpu.make_async_copy(w, buf.at[z, core], o_sem.at[i]) for i, (w, buf) in enumerate(((wa_ref, a_buf), (wb_ref, b_buf)))]
    for load in loads:
        load.start()

    def chip_of(flow, step):
        return lax.rem((z - step if flow == 0 else z + step) + chips, chips)

    def hop(flow, step, kind):
        block = bufs[kind].at[chip_of(flow, step - 1), core]
        return remote(block, block, s_send.at[flow, step - 1, kind], s_recv.at[flow, step - 1, kind], right if flow == 0 else left)

    def landing(flow, step, kind):
        block = bufs[kind].at[chip_of(flow, step), core]
        return remote(block, block, s_send.at[flow, step - 1, kind], s_recv.at[flow, step - 1, kind], right if flow == 0 else left)

    def hand(flow, step, kind):
        block = bufs[kind].at[chip_of(flow, step), core]
        return remote(block, block, p_send.at[flow, step, kind], p_recv.at[flow, step, kind], partner)

    def handed(flow, step, kind):
        block = bufs[kind].at[chip_of(flow, step), 1 - core]
        return remote(block, block, p_send.at[flow, step, kind], p_recv.at[flow, step, kind], partner)

    def add(chip):
        block = jnp.concatenate([a_buf[chip, 0], a_buf[chip, 1]], axis=0)
        qkv_ref[...] += jnp.dot(x_ref[chip], block, preferred_element_type=F32)

    for kind in (0, 1):
        loads[kind].wait()
        for flow in (0, 1):
            hop(flow, 1, kind).start()
        hand(0, 0, kind).start()
    qkv_ref[...] = jnp.zeros_like(qkv_ref)

    def passing(step, flows, onward):
        for kind in (0, 1):
            for flow in flows:
                landing(flow, step, kind).wait_recv()
                if flow in onward:
                    hop(flow, step + 1, kind).start()
                hand(flow, step, kind).start()

    def taking(step, flows):
        for flow in flows:
            for kind in (0, 1):
                handed(flow, step, kind).wait_recv()
            add(chip_of(flow, step))

    passing(1, (0, 1), (0, 1))
    taking(0, (0,))

    def body(step, carry):
        passing(step, (0, 1), (0, 1))
        taking(step - 1, (0, 1))
        return carry

    lax.fori_loop(2, half - 1, body, 0)
    passing(half - 1, (0, 1), (0,))
    taking(half - 2, (0, 1))
    passing(half, (0,), ())
    taking(half - 1, (0, 1))
    taking(half, (0,))

    out = pltpu.make_async_copy(b_buf, wb_out, o_sem.at[2])
    out.start()

    def drained(step, carry):
        for kind in (0, 1):
            for flow in (0, 1):
                hop(flow, step, kind).wait_send()
                hand(flow, step, kind).wait_send()
        return carry

    for kind in (0, 1):
        hand(0, 0, kind).wait_send()
        hop(0, half, kind).wait_send()
        hand(0, half, kind).wait_send()
    lax.fori_loop(1, half, drained, 0)
    out.wait()


def ring(x_blocks, wa, wb, chips):
    rows, wide = wa.shape
    narrow = wb.shape[1]
    half = chips // 2
    any_space = pl.BlockSpec(memory_space=pl.ANY)
    in_vmem = pl.BlockSpec(memory_space=pltpu.VMEM)
    return pl.pallas_call(
        functools.partial(ring_kernel, chips),
        out_shape=(
            jax.ShapeDtypeStruct((x_blocks.shape[1], wide), F32),
            jax.ShapeDtypeStruct((chips, 2, rows, narrow), BF16),
        ),
        in_specs=[in_vmem, any_space, any_space],
        out_specs=(in_vmem, any_space),
        scratch_shapes=[
            pltpu.VMEM((chips, 2, rows, wide), BF16),
            pltpu.VMEM((chips, 2, rows, narrow), BF16),
            pltpu.SemaphoreType.DMA((2, half, 2)),
            pltpu.SemaphoreType.DMA((2, half, 2)),
            pltpu.SemaphoreType.DMA((2, half + 1, 2)),
            pltpu.SemaphoreType.DMA((2, half + 1, 2)),
            pltpu.SemaphoreType.DMA((3,)),
        ],
        compiler_params=pltpu.CompilerParams(collective_id=0, has_side_effects=True),
        name="weights_ring",
    )(x_blocks, wa, wb)


def near_steps(core):
    return (2 - 4 * core, 1 + 0 * core, -1 + 0 * core)


def rows_kernel(chips, x_ref, out_ref, split, pair, s_pair, s_far, r_far, s_near, r_near, s_hand, r_hand):
    z, core, at = place(chips)
    far_count = chips // NEAR
    a, b = lax.div(z, NEAR), lax.rem(z, NEAR)
    half = x_ref.shape[1] // 2
    partner = at(z, 1 - core)
    greet((partner, at(z + NEAR, core), at(z - NEAR, core), at(z + 1, core), at(z - 1, core), at(z + 2, core), at(z - 2, core)))
    split[0] = x_ref[:, :half]
    split[1] = x_ref[:, half:]
    swap = remote(split.at[1 - core], pair.at[core], s_pair.at[0], s_pair.at[1], partner)
    swap.start()
    pair[core] = split[core]
    remote(split.at[core], pair.at[1 - core], s_pair.at[0], s_pair.at[1], partner).wait_recv()
    out_ref[core, b, a] = jnp.concatenate([pair[0], pair[1]], axis=0).astype(BF16)

    limits = (far_count // 2, far_count // 2 - 1)

    def row_of(flow, step, home):
        return lax.rem((home - step if flow == 0 else home + step) + far_count, far_count)

    def far(flow, step):
        block = out_ref.at[core, b, row_of(flow, step - 1, a)]
        return remote(block, block, s_far.at[flow, step - 1], r_far.at[flow, step - 1], at(z + NEAR, core) if flow == 0 else at(z - NEAR, core))

    def far_landing(flow, step):
        block = out_ref.at[core, b, row_of(flow, step, a)]
        return remote(block, block, s_far.at[flow, step - 1], r_far.at[flow, step - 1], partner)

    steps = near_steps(core)
    slots = [(0, 0)] + [(f, s) for s in range(1, limits[0] + 1) for f in (0, 1) if s <= limits[f]]

    def beside(i, k):
        flow, step = slots[k]
        block = out_ref.at[core, b, row_of(flow, step, a)]
        return remote(block, block, s_near.at[i, k], r_near.at[i, k], at(z + steps[i], core))

    def beside_landing(i, k):
        flow, step = slots[k]
        source = lax.rem(z - steps[i] + 2 * chips, chips)
        block = out_ref.at[core, lax.rem(source, NEAR), row_of(flow, step, lax.div(source, NEAR))]
        return remote(block, block, s_near.at[i, k], r_near.at[i, k], partner)

    def hand(i):
        kind = b if i == 3 else lax.rem(z - steps[i] + 2 * chips, NEAR)
        block = out_ref.at[core, kind]
        return remote(block, block, s_hand.at[i], r_hand.at[i], partner)

    def handed(i):
        other = near_steps(1 - core)
        kind = b if i == 3 else lax.rem(z - other[i] + 2 * chips, NEAR)
        block = out_ref.at[1 - core, kind]
        return remote(block, block, s_hand.at[i], r_hand.at[i], partner)

    for k, (flow, step) in enumerate(slots):
        if k == 0:
            far(0, 1).start()
            far(1, 1).start()
        else:
            far_landing(flow, step).wait_recv()
            if step < limits[flow]:
                far(flow, step + 1).start()
        for i in range(3):
            beside(i, k).start()
    hand(3).start()
    for i in range(3):
        for k in range(len(slots)):
            beside_landing(i, k).wait_recv()
        hand(i).start()
    for i in range(4):
        handed(i).wait_recv()
    swap.wait_send()
    for k, (flow, step) in enumerate(slots):
        if k:
            far(flow, step).wait_send()
        for i in range(3):
            beside(i, k).wait_send()
    for i in range(4):
        hand(i).wait_send()


def all_rows(x, chips, number):
    rows, width = x.shape
    half = width // 2
    far_count = chips // NEAR
    in_vmem = pl.BlockSpec(memory_space=pltpu.VMEM)
    return pl.pallas_call(
        functools.partial(rows_kernel, chips),
        out_shape=jax.ShapeDtypeStruct((2, NEAR, far_count, 2 * rows, half), BF16),
        in_specs=[in_vmem],
        out_specs=in_vmem,
        scratch_shapes=[
            pltpu.VMEM((2, rows, half), F32),
            pltpu.VMEM((2, rows, half), F32),
            pltpu.SemaphoreType.DMA((2,)),
            pltpu.SemaphoreType.DMA((2, far_count // 2)),
            pltpu.SemaphoreType.DMA((2, far_count // 2)),
            pltpu.SemaphoreType.DMA((3, far_count)),
            pltpu.SemaphoreType.DMA((3, far_count)),
            pltpu.SemaphoreType.DMA((4,)),
            pltpu.SemaphoreType.DMA((4,)),
        ],
        compiler_params=pltpu.CompilerParams(collective_id=number, has_side_effects=True),
        name="all_rows",
    )(x)


def sums_kernel(chips, p_ref, out_ref, s0, r0, s1, r1, s2, r2, acc, mine, q_send, q_recv, n_send, n_recv, f_send, f_recv, w_sem):
    z, core, at = place(chips)
    far_count = chips // NEAR
    a, b = lax.div(z, NEAR), lax.rem(z, NEAR)
    half = p_ref.shape[3] // 2
    partner = at(z, 1 - core)
    greet((partner, at(z + NEAR, core), at(z - NEAR, core), at(z + 1, core), at(z - 1, core), at(z + 2, core), at(z - 2, core)))
    own_columns = pl.ds(pl.multiple_of(core * half, LANES), half)
    other_columns = pl.ds(pl.multiple_of((1 - core) * half, LANES), half)
    steps = near_steps(core)
    others = near_steps(1 - core)

    def kind_of(move):
        return lax.rem(z + move + chips, NEAR)

    def give(i):
        kind = b if i == 3 else kind_of(others[i])
        return remote(s0.at[kind], r0.at[kind], q_send.at[i], q_recv.at[i], partner)

    def given(i):
        kind = b if i == 3 else kind_of(steps[i])
        return remote(s0.at[kind], r0.at[kind], q_send.at[i], q_recv.at[i], partner)

    def beside(i):
        return remote(s1.at[i], r1.at[i], n_send.at[i], n_recv.at[i], at(z + steps[i], core))

    for i in range(4):
        kind = b if i == 3 else kind_of(others[i])
        s0[kind] = p_ref[kind, :, :, other_columns].astype(BF16)
        give(i).start()
    for i in range(3):
        kind = kind_of(steps[i])
        given(i).wait_recv()
        s1[i] = (p_ref[kind, :, :, own_columns] + r0[kind].astype(F32)).astype(BF16)
        beside(i).start()
    given(3).wait_recv()
    acc[...] = p_ref[b, :, :, own_columns] + r0[b].astype(F32)
    for i in range(3):
        beside(i).wait_recv()
        acc[...] += r1[i].astype(F32)

    limits = (far_count // 2, far_count // 2 - 1)

    def far(flow, step):
        return remote(
            s2.at[flow, step - 1],
            r2.at[flow, step - 1],
            f_send.at[flow, step - 1],
            f_recv.at[flow, step - 1],
            at(z + NEAR, core) if flow == 0 else at(z - NEAR, core),
        )

    for step in range(1, limits[0] + 1):
        for flow in (0, 1):
            if step > limits[flow]:
                continue
            ahead = limits[flow] + 1 - step
            row = lax.rem((a + ahead if flow == 0 else a - ahead) + far_count, far_count)
            value = acc[row]
            if step > 1:
                far(flow, step - 1).wait_recv()
                value = value + r2[flow, step - 2].astype(F32)
            s2[flow, step - 1] = value.astype(BF16)
            far(flow, step).start()
    total = acc[a]
    for flow in (1, 0):
        far(flow, limits[flow]).wait_recv()
        total = total + r2[flow, limits[flow] - 1].astype(F32)
    mine[...] = total
    swap = remote(mine, out_ref.at[core], w_sem.at[0], w_sem.at[1], partner)
    swap.start()
    out_ref[core] = total
    remote(mine, out_ref.at[1 - core], w_sem.at[0], w_sem.at[1], partner).wait_recv()
    swap.wait_send()
    for i in range(4):
        give(i).wait_send()
    for i in range(3):
        beside(i).wait_send()
    for flow in (0, 1):
        for step in range(1, limits[flow] + 1):
            far(flow, step).wait_send()


def owner_sums(partial, chips, number):
    kinds, far_count, rows, width = partial.shape
    half = width // 2
    in_vmem = pl.BlockSpec(memory_space=pltpu.VMEM)
    return pl.pallas_call(
        functools.partial(sums_kernel, chips),
        out_shape=jax.ShapeDtypeStruct((2, rows, half), F32),
        in_specs=[in_vmem],
        out_specs=in_vmem,
        scratch_shapes=[
            pltpu.VMEM((NEAR, far_count, rows, half), BF16),
            pltpu.VMEM((NEAR, far_count, rows, half), BF16),
            pltpu.VMEM((3, far_count, rows, half), BF16),
            pltpu.VMEM((3, far_count, rows, half), BF16),
            pltpu.VMEM((2, far_count // 2, rows, half), BF16),
            pltpu.VMEM((2, far_count // 2, rows, half), BF16),
            pltpu.VMEM((far_count, rows, half), F32),
            pltpu.VMEM((rows, half), F32),
            pltpu.SemaphoreType.DMA((4,)),
            pltpu.SemaphoreType.DMA((4,)),
            pltpu.SemaphoreType.DMA((3,)),
            pltpu.SemaphoreType.DMA((3,)),
            pltpu.SemaphoreType.DMA((2, far_count // 2)),
            pltpu.SemaphoreType.DMA((2, far_count // 2)),
            pltpu.SemaphoreType.DMA((2,)),
        ],
        compiler_params=pltpu.CompilerParams(collective_id=number, has_side_effects=True),
        name="owner_sums",
    )(partial)


def stick_kernel(lengths_ref, q_ref, bias_ref, k_ref, v_ref, o_ref):
    length = lengths_ref[pl.program_id(0)]
    cache_len = k_ref.shape[1]
    chunks = cache_len // LANES
    scores = lax.dot_general(q_ref[0], k_ref[0], (((1,), (1,)), ((), ())), preferred_element_type=F32)
    scores = scores * HEAD_DIM ** (-0.5) + bias_ref[...]
    live = lax.broadcasted_iota(jnp.int32, scores.shape, 1) < length
    soft = jnp.maximum(scores, 0.0) + jnp.log1p(jnp.exp(-jnp.abs(scores)))
    remain = jnp.where(live, -soft, 0.0)
    tall = jnp.concatenate([remain[:, i * LANES : (i + 1) * LANES] for i in range(chunks)], axis=0)
    below = lax.broadcasted_iota(jnp.int32, (LANES, LANES), 0) > lax.broadcasted_iota(jnp.int32, (LANES, LANES), 1)
    ones = below.astype(F32).astype(BF16)
    after = jnp.zeros_like(tall)
    rest = tall
    for _ in range(3):
        part = rest.astype(BF16)
        after = after + jnp.dot(part, ones, preferred_element_type=F32)
        rest = rest - part.astype(F32)
    totals = after[:, 0:1] + tall[:, 0:1]
    later = jnp.zeros((HEADS, 1), F32)
    pieces = [None] * chunks
    for i in reversed(range(chunks)):
        pieces[i] = after[i * HEADS : (i + 1) * HEADS] + later
        later = later + totals[i * HEADS : (i + 1) * HEADS]
    after_sum = jnp.concatenate(pieces, axis=1)
    weights = jnp.where(live, jnp.exp(scores - soft + after_sum), 0.0).astype(BF16)
    mixed = jnp.dot(weights, v_ref[0], preferred_element_type=F32)
    row_kind = lax.rem(lax.broadcasted_iota(jnp.int32, mixed.shape, 0), KV_HEADS)
    own = row_kind == lax.div(lax.broadcasted_iota(jnp.int32, mixed.shape, 1), HEAD_DIM)
    mixed = jnp.where(own, mixed, 0.0)
    for i in range(GROUP):
        o_ref[0, i : i + 1, :] = jnp.sum(mixed[i * KV_HEADS : (i + 1) * KV_HEADS], axis=0, keepdims=True)


def stick_attend(queries, lengths, cache_key, cache_value, query_gain, head_bias):
    rows = queries.shape[0]
    cache_len, width = cache_key.shape[1:]
    normed = rms_scaled(queries.reshape(rows, HEADS, HEAD_DIM), query_gain).astype(BF16)
    by_member = normed.reshape(rows, KV_HEADS, GROUP, HEAD_DIM).transpose(0, 2, 1, 3)
    eye = jnp.eye(KV_HEADS, dtype=BF16)
    spread = by_member[:, :, :, None, :] * eye[None, None, :, :, None]
    spread = spread.reshape(rows, HEADS, width)
    bias = head_bias.reshape(KV_HEADS, GROUP).T.reshape(HEADS, 1)
    out = pl.pallas_call(
        stick_kernel,
        grid_spec=pltpu.PrefetchScalarGridSpec(
            num_scalar_prefetch=1,
            grid=(rows,),
            in_specs=[
                pl.BlockSpec((1, HEADS, width), lambda i, n: (i, 0, 0)),
                pl.BlockSpec((HEADS, 1), lambda i, n: (0, 0)),
                pl.BlockSpec((1, cache_len, width), lambda i, n: (i, 0, 0)),
                pl.BlockSpec((1, cache_len, width), lambda i, n: (i, 0, 0)),
            ],
            out_specs=pl.BlockSpec((1, GROUP, width), lambda i, n: (i, 0, 0)),
        ),
        out_shape=jax.ShapeDtypeStruct((rows, GROUP, width), F32),
        name="stick_attend",
    )(lengths, spread, bias, cache_key, cache_value)
    out = out.reshape(rows, GROUP, KV_HEADS, HEAD_DIM).transpose(0, 2, 1, 3)
    return out.reshape(rows, HEADS * HEAD_DIM).astype(BF16)


def local(
    chips,
    tokens,
    lengths,
    cache_key,
    cache_value,
    routes,
    route_logits,
    mix_gain,
    query_gain,
    key_gain,
    head_bias,
    w_query,
    w_key,
    w_value,
    w_out,
    ffn_gain,
    w_gate,
    w_up,
    w_down,
):
    rows, width = tokens.shape
    key_width = w_key.shape[1]
    query_width = w_query.shape[1]
    core = lax.rem(lax.axis_index(EP), 2)
    as_float = tokens.astype(F32)
    normed = rms_scaled(as_float, mix_gain).astype(BF16)
    x_blocks = normed.reshape(rows, chips, width // chips).transpose(1, 0, 2)
    wa = jnp.concatenate([w_query, w_key, w_value], axis=1)
    qkv, w_out_all = ring(x_blocks, wa, w_out.T, chips)
    queries = qkv[:, :query_width]
    fresh_key = qkv[:, query_width : query_width + key_width]
    fresh_value = qkv[:, query_width + key_width :]
    new_key = rms_scaled(fresh_key.reshape(rows, KV_HEADS, HEAD_DIM), key_gain)
    new_key = new_key.reshape(rows, key_width).astype(BF16)
    new_value = fresh_value.astype(BF16)
    attended = stick_attend(queries, lengths, cache_key, cache_value, query_gain, head_bias)
    w_out_all = w_out_all.reshape(width, w_out.shape[0])
    mixed = as_float + lax.dot_general(attended, w_out_all, (((1,), (1,)), ((), ())), preferred_element_type=F32)
    expert_in = rms_scaled(mixed, ffn_gain)

    gates = route_weights(routes, route_logits)
    coarse = lax.reduce_precision(gates, 8, 7)
    half = width // 2
    room = ((0, 0), (0, LANES - EXPERTS))
    x = jnp.concatenate([expert_in[:, :half], jnp.pad(coarse, room), expert_in[:, half:], jnp.pad(gates - coarse, room)], axis=1)
    every = all_rows(x, chips, 1)
    batch = chips * 2 * rows
    every = every.reshape(2, batch, half + LANES)
    ff_share = w_gate.shape[1]
    my_expert = lax.axis_index(EP) // (FF // ff_share)
    my_gate = lax.dynamic_slice_in_dim(every[:, :, half:].astype(F32).sum(0), my_expert, 1, 1)
    input_rows = jnp.concatenate([every[0, :, :half], every[1, :, :half]], axis=1)
    gate_value = jnp.dot(input_rows, w_gate, preferred_element_type=F32)
    up_value = jnp.dot(input_rows, w_up, preferred_element_type=F32)
    hidden = (jax.nn.silu(gate_value) * up_value * my_gate).astype(BF16)
    partial = jnp.dot(hidden, w_down, preferred_element_type=F32)
    sums = owner_sums(partial.reshape(NEAR, chips // NEAR, 2 * rows, width), chips, 2)
    sums = lax.dynamic_slice_in_dim(sums, core * rows, rows, 1)
    sums = sums.transpose(1, 0, 2).reshape(rows, width)
    return ((mixed + sums).astype(BF16), new_key, new_value)


def solution(mesh):
    chips = mesh.shape[EP] // 2
    both = ("grp", EP)
    in_specs = (
        P(both, None),
        P(both),
        P(both, None, None),
        P(both, None, None),
        P(both, None),
        P(both, None),
        P(),
        P(),
        P(),
        P(),
        P(EP, None),
        P(EP, None),
        P(EP, None),
        P(None, EP),
        P(),
        P(None, EP),
        P(None, EP),
        P(EP, None),
    )
    out_specs = (P(both, None), P(both, None), P(both, None))
    return jax.shard_map(functools.partial(local, chips), mesh=mesh, in_specs=in_specs, out_specs=out_specs, check_vma=False)
```

time: 722 us -> 201 us (0.28)
  the two profiles are of different devices: /device:TPU:38 before, /device:TPU:37 now
where the time goes in v1:
time: 201 us; the launch traced here: 200 us
  Pallas kernels  171 us (85%)
  other arithmetic  10.6 us (5%)
  matrix products  9.31 us (5%)
  local copies, waits for them, and re-layouts  7.45 us (4%)
    pallas_call x1, Pallas kernels, ring(): pl.pallas_call(functools.partial(ring_kernel, chips), out_shape=(jax.Shap...  97.8 us
    pallas_call x1, Pallas kernels, owner_sums(): pl.pallas_call(functools.partial(sums_kernel, chips), out_shape=jax.Shape...  34.5 us
    pallas_call x1, Pallas kernels, all_rows(): pl.pallas_call(functools.partial(rows_kernel, chips), out_shape=jax.Shape...  33 us
    pallas_call x1, Pallas kernels, stick_attend(): pl.pallas_call(stick_kernel, grid_spec=pltpu.PrefetchScalarGridSpec(num_s...  6.12 us
    dot_general x1, matrix products, local(): partial = jnp.dot(hidden, w_down, preferred_element_type=F32)  5.13 us

profile of v1, /device:TPU:37, one launch (start us, length us, event | category | flops | bytes accessed | tf_op | source)
XLA Modules:
  0.0 199.7 jit_solution(2683285728294021010)
XLA Ops:
  0.6 1.0 fusion.13
  1.6 0.8 fusion.15
  2.5 0.6 copy.37
  3.2 1.5 pad_maximum_fusion.4.wa_ref
  4.7 97.8 %weights_ring.1 = (f32[4,1536]{1,0:T(4,128)}, bf16[32,2,32,1024]{3,2,1,0:T(8,128)(2,1)}) custom-call(bf16[32,4,64]{2,1,0:T(4,128)(2,1)} %bitcast.38, bf16[32,1536]{1,0:T(8,128)(2,1)} %pad_maximum_fusion.4.wa_ref, bf16[32,1024]{1,0:T(8,128)(2,1)} %bitcast.39), custom_call_target="tpu_custom_call" | custom-call | tf_op jit(solution)/shard_map/weights_ring/pallas_call | solution.py:161
  102.5 0.7 slice_multiply_fusion.1
  103.6 0.7 fusion.16
  105.3 0.7 reshape.100
  106.1 0.7 reshape.106.bias_ref
  106.8 6.1 %stick_attend.1 = f32[4,4,256]{2,1,0:T(4,128)} custom-call(s32[4]{0:T(128)} %lengths_ref.1, bf16[4,16,256]{2,1,0:T(8,128)(2,1)} %broadcast_multiply_fusion.q_ref, f32[16,1]{1,0:T(8,128)} %reshape.106.bias_ref, bf16[4,1024,256]{2,1,0:T(8,128)(2,1)} %k_ref.1, bf16[4,1024,256]{2,1,0:T(8,128)(2,1)} %v_ref.1), custom_call_target="tpu_custom_call" | custom-call | tf_op jit(solution)/shard_map/stick_attend/pallas_call | solution.py:450
  113.0 0.7 convert_element_type.49
  113.9 3.5 %multiply_reduce_fusion = (f32[4]{0:T(128)S(1)}, f32[4,2048]{1,0:T(4,128)S(1)}) fusion(bf16[4,1024]{1,0:T(4,128)(2,1)S(1)} %convert_element_type.52, bf16[2048,1024]{1,0:T(8,128)(2,1)} %bitcast.35, bf16[4,2048]{1,0:T(4,128)(2,1)S(1)} %copy-done.1), kind=kOutput, calls=%fused_computation.34 | convolution fusion | flops 16809980 | bytes 4251664 | tf_op jit(solution)/shard_map/dot_general | solution.py:508
  117.6 0.6 select_maximum_fusion.x_ref
  118.2 33.0 %all_rows.1 = bf16[2,4,8,8,1152]{4,3,2,1,0:T(8,128)(2,1)} custom-call(f32[4,2304]{1,0:T(4,128)} %select_maximum_fusion.x_ref), custom_call_target="tpu_custom_call" | custom-call | tf_op jit(solution)/shard_map/all_rows/pallas_call | solution.py:272
  151.3 1.4 slice_bitcast_fusion.1
  153.1 0.7 fusion.3
  153.7 0.9 convert_reduce_fusion
  154.9 5.1 %fusion.2 = f32[256,2048]{1,0:T(8,128)} fusion(bf16[448,2048]{1,0:T(8,128)(2,1)S(1)} %copy-done, bf16[2048,448]{0,1:T(8,128)(2,1)} %param.34, bf16[256,1024]{1,0:T(8,128)(2,1)S(1)} %get-tuple-element.8, bf16[256,1024]{1,0:T(8,128)(2,1)S(1)} %get-tuple-element.7, f32[256,448]{0,1:T(8,128)S(1)} %fusion.3, f32[256]{0:T(256)S(1)} %dynamic-slice_reduce_fusion), kind=kOutput, calls=%fused_computation.4 | convolution fusion | flops 942424064 | bytes 7275520 | tf_op jit(solution)/shard_map/dot_general | solution.py:526
  160.0 34.5 %owner_sums.1 = f32[2,8,1024]{2,1,0:T(8,128)} custom-call(f32[4,8,8,2048]{3,2,1,0:T(8,128)} %bitcast.36), custom_call_target="tpu_custom_call" | custom-call | tf_op jit(solution)/shard_map/owner_sums/pallas_call | solution.py:380
  194.6 0.9 constant_dynamic-slice_fusion
  195.4 0.6 add_convert_fusion
  196.0 0.7 slice_multiply_fusion
  197.1 1.3 multiply_convert_fusion.1
  198.4 1.3 slice.70
  (46 shorter events, 2.9 us)
Async XLA Ops:
  0.6 154.2 %copy-start = (bf16[448,2048]{1,0:T(8,128)(2,1)S(1)}, bf16[448,2048]{1,0:T(8,128)(2,1)}, u32[]{:S(2)}) copy-start(bf16[448,2048]{1,0:T(8,128)(2,1)} %param.35) | copy-start | bytes 5505028
  106.8 7.0 %copy-start.1 = (bf16[4,2048]{1,0:T(4,128)(2,1)S(1)}, bf16[4,2048]{1,0:T(4,128)(2,1)}, u32[]{:S(2)}) copy-start(bf16[4,2048]{1,0:T(4,128)(2,1)} %param.18) | copy-start | bytes 49156
  113.9 3.5 %copy-start.3 = (f32[4,2]{0,1:T(2,128)S(1)}, f32[4,2]{0,1:T(2,128)}, u32[]{:S(2)}) copy-start(f32[4,2]{0,1:T(2,128)} %param.23) | copy-start | bytes 100
  113.9 3.6 %copy-start.4 = (s32[4,2]{0,1:T(2,128)S(1)}, s32[4,2]{0,1:T(2,128)}, u32[]{:S(2)}) copy-start(s32[4,2]{0,1:T(2,128)} %param.22) | copy-start | bytes 100
  113.9 3.7 %copy-start.2 = (f32[2048]{0:T(1024)S(1)}, f32[2048]{0:T(1024)}, u32[]{:S(2)}) copy-start(f32[2048]{0:T(1024)} %param.32) | copy-start | bytes 24580
  151.2 1.8 copy-start.6
  160.0 37.0 %copy-start.5 = (f32[64]{0:T(128)S(1)}, f32[64]{0:T(128)}, u32[]{:S(2)}) copy-start(f32[64]{0:T(128)} %param.26) | copy-start | bytes 772
